TPU v7x, 32 devices: a whole 2x2x4 slice. The times are simulated.
32 devices in a mesh: sp: 8 (over z, y), dp: 4 (over x, core).
Axes of the slice: x: 2, y: 2, z: 4, core: 2. Of those that a mesh axis runs over, the one named last changes fastest.
Arguments:
- query: bfloat16 [4, 1536, 3072], P('dp', 'sp'), may hold values from -18 to 18
- latent: bfloat16 [4, 1536, 1024], P('dp', 'sp'), may hold values from -6 to 6
- rope_key: bfloat16 [4, 1536, 32], P('dp', 'sp'), may hold values from -5 to 5
- latent_norm_gain: float32 [1024], replicated, may hold values from 0.1 to 1.9
- key_up_matrix: bfloat16 [2048, 1024], P('dp'), may hold values from -0.1875 to 0.1875
- value_up_matrix: bfloat16 [2048, 1024], P('dp'), may hold values from -0.1875 to 0.1875
- out_grad: bfloat16 [4, 1536, 2048], P('dp', 'sp'), may hold values from -6 to 6
Outputs:
- query_grad: bfloat16 [4, 1536, 3072], P('dp', 'sp')
- latent_grad: float32 [4, 1536, 1024], P('dp', 'sp')
- rope_key_grad: float32 [4, 1536, 32], P('dp', 'sp')
- key_weight_grad: float32 [2048, 1024], P('dp')
- value_weight_grad: float32 [2048, 1024], P('dp')
- gain_grad: float32 [1024], replicated
All inputs are finite; a program needn't handle non-finite values.
Results may differ from a plain program's by a relative error of at most 0.011.
Values may be sent and summed in bfloat16 or wider, within the bound.
A program may use at most 256 MiB of HBM per device.

v0:
```python
import jax
import jax.numpy as jnp
from jax import lax
from jax.sharding import PartitionSpec as P

ATTENTION_HEADS = 32
PLAIN_HEAD_WIDTH = 64
ROPE = 32
VALUE_HEAD_WIDTH = 64
SPAN = 64
eps = 1e-06
rope_base = 10000.0


def rotate(values, cosine, sine):
    half = values.shape[-1] // 2
    first = values[..., :half]
    second = values[..., half:]
    return jnp.concatenate(
        [first * cosine - second * sine, second * cosine + first * sine], axis=-1
    )


def angles(length, width):
    inverse = 1.0 / rope_base ** (jnp.arange(0, width, 2, dtype=jnp.float32) / width)
    turned = jnp.arange(length, dtype=jnp.float32)[:, None] * inverse[None, :]
    return (jnp.cos(turned), jnp.sin(turned))


def attend_backward(arrived, rope_full):
    f32 = jnp.float32
    bf16 = jnp.bfloat16
    length = arrived.shape[0]
    local_heads = arrived.shape[1]
    width = PLAIN_HEAD_WIDTH + ROPE
    scale = width ** (-0.5)
    block = 512
    cosine, sine = angles(length, ROPE)
    neg = jnp.finfo(f32).min
    q_nope = arrived[:, :, :PLAIN_HEAD_WIDTH]
    q_rope = rotate(
        arrived[:, :, PLAIN_HEAD_WIDTH:width].astype(f32), cosine[:, None, :], sine[:, None, :]
    ).astype(bf16)
    key_nope = arrived[:, :, width : width + PLAIN_HEAD_WIDTH]
    values = arrived[:, :, width + PLAIN_HEAD_WIDTH : width + PLAIN_HEAD_WIDTH + VALUE_HEAD_WIDTH]
    d_out = arrived[:, :, width + PLAIN_HEAD_WIDTH + VALUE_HEAD_WIDTH :]
    k_rope = rotate(rope_full.astype(f32), cosine, sine).astype(bf16)
    dk_nope = jnp.zeros((length, local_heads, PLAIN_HEAD_WIDTH), f32)
    dk_rope = jnp.zeros((length, ROPE), f32)
    d_vals = jnp.zeros((length, local_heads, VALUE_HEAD_WIDTH), f32)
    dq_parts = []
    for begin in range(0, length, block):
        end = begin + block
        qn = q_nope[begin:end]
        qr = q_rope[begin:end]
        go = d_out[begin:end]
        scores = jnp.einsum("qhd,khd->hqk", qn, key_nope[:end], preferred_element_type=f32)
        scores = (
            scores + jnp.einsum("qhd,kd->hqk", qr, k_rope[:end], preferred_element_type=f32)
        ) * scale
        q_seg = jnp.arange(begin, end) // SPAN
        k_seg = jnp.arange(end) // SPAN
        allowed = k_seg[None, :] <= q_seg[:, None]
        scores = jnp.where(allowed[None], scores, neg)
        probs = jax.nn.softmax(scores, axis=-1)
        d_probs = jnp.einsum("qhd,khd->hqk", go, values[:end], preferred_element_type=f32)
        d_scores = probs * (d_probs - jnp.sum(probs * d_probs, axis=-1, keepdims=True))
        ds_b = d_scores.astype(bf16)
        p_b = probs.astype(bf16)
        dq_n = jnp.einsum("hqk,khd->qhd", ds_b, key_nope[:end], preferred_element_type=f32) * scale
        dq_r = jnp.einsum("hqk,kd->qhd", ds_b, k_rope[:end], preferred_element_type=f32) * scale
        dq_r = rotate(dq_r, cosine[begin:end, None, :], -sine[begin:end, None, :])
        dq_parts.append(jnp.concatenate([dq_n, dq_r], axis=-1).astype(bf16))
        dk_nope = dk_nope.at[:end].add(
            jnp.einsum("hqk,qhd->khd", ds_b, qn, preferred_element_type=f32) * scale
        )
        dk_rope = dk_rope.at[:end].add(
            jnp.einsum("hqk,qhd->kd", ds_b, qr, preferred_element_type=f32) * scale
        )
        d_vals = d_vals.at[:end].add(
            jnp.einsum("hqk,qhd->khd", p_b, go, preferred_element_type=f32)
        )
    query_part = jnp.concatenate(dq_parts, axis=0)
    grads = jnp.concatenate([query_part, dk_nope.astype(bf16), d_vals.astype(bf16)], axis=-1)
    return (grads, rotate(dk_rope, cosine, -sine))


def local(query, latent, rope_key, latent_norm_gain, key_up_matrix, value_up_matrix, out_grad):
    f32 = jnp.float32
    bf16 = jnp.bfloat16
    tokens = latent.shape[1]
    width = PLAIN_HEAD_WIDTH + ROPE
    head_cols = ATTENTION_HEADS * PLAIN_HEAD_WIDTH
    lat = latent[0].astype(f32)
    inv_rms = lax.rsqrt(jnp.mean(lat * lat, axis=-1, keepdims=True) + eps)
    normed = lat * inv_rms
    nlat = (normed * latent_norm_gain).astype(bf16)
    stacked = jnp.stack([key_up_matrix, value_up_matrix])
    whole = lax.all_gather(stacked, "dp", axis=1, tiled=True)
    kv_tok = jnp.einsum("tc,gnc->tgn", nlat, whole, preferred_element_type=f32).astype(bf16)
    heads_query = query[0].reshape(tokens, ATTENTION_HEADS, width)
    key_nope = kv_tok[:, 0].reshape(tokens, ATTENTION_HEADS, PLAIN_HEAD_WIDTH)
    values = kv_tok[:, 1].reshape(tokens, ATTENTION_HEADS, VALUE_HEAD_WIDTH)
    d_out = out_grad[0].reshape(tokens, ATTENTION_HEADS, VALUE_HEAD_WIDTH)
    packed = jnp.concatenate([heads_query, key_nope, values, d_out], axis=2)
    arrived = lax.all_to_all(packed, "sp", split_axis=1, concat_axis=0, tiled=True)
    rope_full = lax.all_gather(rope_key[0], "sp", axis=0, tiled=True)
    grads_heads, rope_full_grad = attend_backward(arrived, rope_full)
    returned = lax.all_to_all(grads_heads, "sp", split_axis=0, concat_axis=1, tiled=True)
    rope_grad = lax.psum_scatter(rope_full_grad, "sp", scatter_dimension=0, tiled=True)
    query_grad = returned[:, :, :width].reshape(tokens, ATTENTION_HEADS * width)
    key_cols = returned[:, :, width : width + PLAIN_HEAD_WIDTH].reshape(tokens, head_cols)
    value_cols = returned[:, :, width + PLAIN_HEAD_WIDTH :].reshape(tokens, head_cols)
    dkv = jnp.stack([key_cols, value_cols], axis=1)
    d_nlat = jnp.einsum("tgn,gnc->tc", dkv, whole, preferred_element_type=f32)
    latents_all = lax.all_gather(nlat[None], "dp", axis=0, tiled=True)
    columns = lax.all_to_all(dkv[None], "dp", split_axis=3, concat_axis=0, tiled=True)
    partial_value = jnp.einsum("stgr,stc->grc", columns, latents_all, preferred_element_type=f32)
    weight_grads = lax.psum(partial_value, "sp")
    gain_grad = lax.psum(jnp.sum(d_nlat * normed, axis=0), ("sp", "dp"))
    scaled = d_nlat * latent_norm_gain
    latent_grad = inv_rms * (scaled - normed * jnp.mean(scaled * normed, axis=-1, keepdims=True))
    return (
        query_grad[None],
        latent_grad[None],
        rope_grad[None],
        weight_grads[0],
        weight_grads[1],
        gain_grad,
    )


def solution(mesh):
    in_specs = (
        P("dp", "sp", None),
        P("dp", "sp", None),
        P("dp", "sp", None),
        P(),
        P("dp", None),
        P("dp", None),
        P("dp", "sp", None),
    )
    out_specs = (
        P("dp", "sp", None),
        P("dp", "sp", None),
        P("dp", "sp", None),
        P("dp", None),
        P("dp", None),
        P(),
    )
    return jax.shard_map(local, mesh=mesh, in_specs=in_specs, out_specs=out_specs, check_vma=False)
```

profile of v0, /device:TPU:0, one launch (start us, length us, event | category | flops | bytes accessed | tf_op | source)
XLA Modules:
  0.0 738.0 jit_solution(6265751976223707838)
XLA Ops:
  16.4 55.1 %all-gather.4.cloned.1.call-done = bf16[2,2048,1024]{2,1,0:T(8,128)(2,1)} async-done(((bf16[2,512,1024]{2,1,0:T(8,128)(2,1)}), bf16[2,2048,1024]{2,1,0:T(8,128)(2,1)}) %all-gather.4.cloned.1.call-update) | async-done | bytes 8388624 | tf_op jit(solution)/shard_map/all_gather | solution.py:99
  71.5 6.2 convolution_convert_fusion
  87.8 5.6 pad_maximum_fusion
  93.4 4.0 copy.97
  97.4 5.6 all-to-all-start
  103.2 126.8 %all-gather = bf16[1,1536,32]{2,0,1:T(2,128)(2,1)S(1)} all-gather(bf16[1,192,32]{2,0,1:T(2,128)(2,1)S(1)} %copy.99), channel_id=2, replica_groups=mesh['sp'=8,'dp'=4] {'sp'}, dimensions={1}, use_global_device_ids=true | all-gather | bytes 110592 | tf_op jit(solution)/shard_map/all_gather | solution.py:107
  236.4 8.3 %copy.98 = bf16[8,192,4,288]{1,0,3,2:T(8,128)(2,1)} copy(bf16[8,192,4,288]{3,1,2,0:T(8,128)(2,1)} %bitcast.8) | data formatting | bytes 7077888 | tf_op jit(solution)/shard_map/all_to_all | solution.py:106
  244.7 6.9 all_to_all.42
  258.0 5.4 fusion.43
  283.7 9.7 %multiply_convert_fusion.1 = bf16[4,512,1024]{2,1,0:T(8,128)(2,1)S(1)} fusion(f32[4,512,1024]{2,1,0:T(8,128)S(1)} %get-tuple-element.177, f32[4,512]{1,0:T(4,128)S(1)} %get-tuple-element.176, f32[4,512,1024]{2,1,0:T(8,128)S(1)} %get-tuple-element.171, f32[4,512]{1,0:T(4,128)S(1)} %get-tuple-element.170), kind=kLoop, calls=%fused_computation.12 | loop fusion | flops 8388608 | bytes 20987904 | tf_op jit(solution)/shard_map/convert_element_type | solution.py:68
  300.5 8.5 %fusion.4 = f32[4,512,1536]{2,1,0:T(8,128)} fusion(f32[1536,512,4]{0,1,2:T(8,128)S(1)} %fusion.114, pred[512,1536]{1,0:T(8,128)(4,1)S(1)} %copy-done.13, bf16[1536,4,288]{0,2,1:T(8,128)(2,1)} %copy-done.3), kind=kOutput, calls=%fused_computation.5 | convolution fusion | flops 412090368 | bytes 27000832 | tf_op jit(solution)/shard_map/qhd,khd->hqk/dot_general | solution.py:57
  309.1 14.9 %fusion.154 = (f32[4,512]{1,0:T(4,128)S(1)}, f32[4,512,1536]{2,1,0:T(8,128)}) fusion(f32[4,512,1536]{2,1,0:T(8,128)} %fusion.4), kind=kOutput, calls=%fused_computation.226 | output fusion | flops 6292991 | bytes 25174016 | tf_op jit(solution)/shard_map/sub | solution.py:65
  323.9 11.8 %multiply_reduce_fusion = (f32[4,512]{1,0:T(4,128)S(1)}, f32[4,512,1536]{2,1,0:T(8,128)}) fusion(f32[4,512,1536]{2,1,0:T(8,128)} %get-tuple-element.173, f32[4,512]{1,0:T(4,128)S(1)} %get-tuple-element.172, bf16[1536,4,288]{0,2,1:T(8,128)(2,1)} %copy-done.3), kind=kOutput, calls=%fused_computation.7 | convolution fusion | flops 412088320 | bytes 26230784 | tf_op jit(solution)/shard_map/qhd,khd->hqk/dot_general | solution.py:66
  335.7 6.0 multiply_convert_fusion
  341.8 4.5 fusion.52
  351.6 11.2 %fusion.37 = f32[1536,4,64]{0,2,1:T(8,128)} fusion(f32[1536,4,64]{0,2,1:T(8,128)} %scatter-add.24, bf16[1536,4,288]{0,2,1:T(8,128)(2,1)} %copy-done.3, f32[4,512]{1,0:T(4,128)S(1)} %get-tuple-element.170, f32[4,512,1024]{2,1,0:T(8,128)} %copy-done.2), kind=kOutput, calls=%fused_computation.53 | convolution fusion | flops 274992128 | bytes 19144704 | tf_op jit(solution)/shard_map/hqk,qhd->khd/dot_general | solution.py:81
  362.8 4.4 fusion.42
  367.2 13.7 %fusion.22 = bf16[1536,4,64]{0,2,1:T(8,128)(2,1)} fusion(f32[1536,4,64]{0,2,1:T(8,128)} %fusion.37, bf16[1536,4,288]{0,2,1:T(8,128)(2,1)} %copy-done.3, f32[4,512]{1,0:T(4,128)S(1)} %get-tuple-element.172, f32[4,512,1536]{2,1,0:T(8,128)} %fusion.4), kind=kOutput, calls=%fused_computation.36 | convolution fusion | flops 412880384 | bytes 27795456 | tf_op jit(solution)/shard_map/hqk,qhd->khd/dot_general | solution.py:81
  381.0 4.6 fusion.21
  388.8 5.8 copy.107
  394.6 4.6 all-to-all-start.1
  401.9 64.4 %all-to-all-done.1 = bf16[1536,4,224]{2,1,0:T(4,128)(2,1)} async-done(((bf16[1536,4,224]{2,1,0:T(4,128)(2,1)}), bf16[1536,4,224]{2,1,0:T(4,128)(2,1)}, u32[]{:S(2)}, u32[]{:S(2)}) %all-to-all-start.1) | async-done | bytes 2752544 | tf_op jit(solution)/shard_map/all_to_all | solution.py:109
  483.8 6.1 copy.116
  489.8 4.4 all-to-all-start.2
  503.7 16.3 %all-to-all-done.2 = bf16[1,192,2,2048]{1,2,0,3:T(2,128)(2,1)} async-done(((bf16[1,192,2,2048]{1,2,0,3:T(2,128)(2,1)}), bf16[1,192,2,2048]{1,2,0,3:T(2,128)(2,1)}, u32[]{:S(2)}, u32[]{:S(2)}) %all-to-all-start.2) | async-done | bytes 1572896 | tf_op jit(solution)/shard_map/all_to_all | solution.py:117
  520.0 6.0 copy.118
  526.0 5.7 convolution_bitcast_fusion.1
  531.7 34.6 %reduce-scatter.4.cloned.1.call-done = f32[192,32]{1,0:T(8,128)} async-done(((f32[1536,32]{1,0:T(8,128)}), f32[192,32]{1,0:T(8,128)}) %reduce-scatter.4.cloned.1.call-update) | async-done | bytes 24592
  572.2 6.3 fusion.72
  578.5 44.0 %psum.15 = f32[1024]{0:T(1024)} all-reduce(f32[1024]{0:T(1024)S(1)} %get-tuple-element.138), channel_id=1, replica_groups=mesh['sp'=8,'dp'=4] {'sp','dp'}, use_global_device_ids=true, to_apply=%region_14.15 | all-reduce | flops 1024 | bytes 8192 | tf_op jit(solution)/shard_map/psum | solution.py:120
  623.6 102.6 %all-reduce.5.cloned.1.call-done = f32[2,512,1024]{2,1,0:T(8,128)} async-done(((f32[2,512,1024]{2,1,0:T(8,128)}), f32[2,512,1024]{2,1,0:T(8,128)}) %all-reduce.5.cloned.1.call-update) | async-done | bytes 4194320 | tf_op jit(solution)/shard_map/psum | solution.py:119
  726.2 4.8 slice_bitcast_fusion
  (184 shorter events, 104.2 us)
Async XLA Ops:
  7.2 64.3 %all-gather.4.cloned.1.call-start = ((), (), s32[]{:S(2)}) async-start(), calls=%async_computation.4 | async-start | bytes 10485760 | tf_op jit(solution)/shard_map/all_gather | solution.py:99
  10.3 5.9 copy-start.10
  10.4 61.1 %copy-start.41 = (f32[1024]{0:T(1024)S(1)}, f32[1024]{0:T(1024)}, u32[]{:S(2)}) copy-start(f32[1024]{0:T(1024)} %param.34) | copy-start | bytes 12292
  16.4 55.1 %copy-start.44 = (f32[192]{0:T(256)}, f32[192]{0:T(256)S(1)}, u32[]{:S(2)}) copy-start(f32[192]{0:T(256)S(1)} %add_rsqrt_fusion) | copy-start | bytes 2308
  97.4 5.7 copy-start.43
  97.4 139.0 %all-to-all-start = ((bf16[192,32,288]{2,0,1:T(8,128)(2,1)}), bf16[192,32,288]{2,0,1:T(8,128)(2,1)}, u32[]{:S(2)}, u32[]{:S(2)}) async-start(bf16[192,32,288]{2,0,1:T(8,128)(2,1)} %copy.97), calls=%async_computation | async-start | bytes 9437184 | tf_op jit(solution)/shard_map/all_to_all | solution.py:106
  251.6 11.8 %copy-start.3 = (bf16[1536,4,288]{0,2,1:T(8,128)(2,1)}, bf16[1536,4,288]{0,2,1:T(8,128)(2,1)S(1)}, u32[]{:S(2)}) copy-start(bf16[1536,4,288]{0,2,1:T(8,128)(2,1)S(1)} %all_to_all.42) | copy-start | bytes 10616836
  268.0 5.0 copy-start.7
  268.0 5.0 copy-start.9
  293.4 5.2 copy-start.1
  323.9 11.8 %slice-start = ((s8[12582912]{0:T(1024)(128)(4,1)}), s8[4194304]{0:T(1024)(128)(4,1)S(1)}, s32[]{:S(2)}) async-start(s8[12582912]{0:T(1024)(128)(4,1)} %bitcast.187), calls=%async_computation.8 | async-start | bytes 8388608
  323.9 11.8 %slice-start.1 = ((s8[12582912]{0:T(1024)(128)(4,1)}), s8[4194304]{0:T(1024)(128)(4,1)S(1)}, s32[]{:S(2)}) async-start(s8[12582912]{0:T(1024)(128)(4,1)} %bitcast.187), calls=%async_computation.9 | async-start | bytes 8388608
  323.9 11.8 %slice-start.2 = ((s8[12582912]{0:T(1024)(128)(4,1)}), s8[4194304]{0:T(1024)(128)(4,1)S(1)}, s32[]{:S(2)}) async-start(s8[12582912]{0:T(1024)(128)(4,1)} %bitcast.187), calls=%async_computation.10 | async-start | bytes 8388608
  341.8 7.1 copy-start
  380.9 4.8 copy-start.22
  380.9 4.8 copy-start.37
  380.9 4.8 copy-start.38
  380.9 4.9 copy-start.23
  380.9 4.9 copy-start.35
  380.9 4.9 copy-start.36
  380.9 4.9 copy-start.25
  381.0 4.9 copy-start.26
  381.0 4.9 copy-start.27
  381.0 4.9 copy-start.33
  394.6 4.9 copy-start.11
  394.6 4.9 copy-start.42
  394.6 4.9 copy-start.45
  394.6 71.6 %all-to-all-start.1 = ((bf16[1536,4,224]{2,1,0:T(4,128)(2,1)}), bf16[1536,4,224]{2,1,0:T(4,128)(2,1)}, u32[]{:S(2)}, u32[]{:S(2)}) async-start(bf16[1536,4,224]{2,1,0:T(4,128)(2,1)} %copy.107), calls=%async_computation.1 | async-start | bytes 6291456 | tf_op jit(solution)/shard_map/all_to_all | solution.py:109
  399.2 126.8 %all-gather.6.cloned.1.call-start = ((), (), s32[]{:S(2)}) async-start(), calls=%async_computation.5 | async-start | bytes 1966080 | tf_op jit(solution)/shard_map/all_gather | solution.py:116
  489.8 30.2 %all-to-all-start.2 = ((bf16[1,192,2,2048]{1,2,0,3:T(2,128)(2,1)}), bf16[1,192,2,2048]{1,2,0,3:T(2,128)(2,1)}, u32[]{:S(2)}, u32[]{:S(2)}) async-start(bf16[1,192,2,2048]{1,2,0,3:T(2,128)(2,1)} %copy.116), calls=%async_computation.2 | async-start | bytes 4194304 | tf_op jit(solution)/shard_map/all_to_all | solution.py:117
  494.3 72.0 %reduce-scatter.4.cloned.1.call-start = ((), (), s32[]{:S(2)}) async-start(), calls=%async_computation.7 | async-start | bytes 884736
  503.6 222.6 %all-reduce.5.cloned.1.call-start = ((), (), s32[]{:S(2)}) async-start(), calls=%async_computation.6 | async-start | bytes 8388608 | tf_op jit(solution)/shard_map/psum | solution.py:119
  (26 other events, 64.0 us)
Sparse Core Ops, SparseCore 0:
  10.5 60.9 all-gather.3
  401.6 19.9 all-gather.5
  503.8 62.4 reduce-scatter.3
  569.8 156.3 all-reduce.4
where the time goes:
time: 747 us; the launch traced here: 738 us
  waiting for transfers between devices  273 us (37%)
  blocking collectives  171 us (23%)
  matrix products  118 us (16%)
  local copies, waits for them, and re-layouts  87 us (12%)
  other arithmetic  59.6 us (8%)
  starting transfers between devices  15.1 us (2%)
  between operations  15 us (2%)
    all_gather x1, blocking collectives, local(): rope_full = lax.all_gather(rope_key[0], 'sp', axis=0, tiled=True)  127 us
    psum x1, waiting for transfers between devices, local(): weight_grads = lax.psum(partial_value, 'sp')  103 us
    all_to_all x1, waiting for transfers between devices, local(): lax.all_to_all(grads_heads, 'sp', split_axis=0, concat_axis=1, tiled=True)  64.4 us
    all_gather x1, waiting for transfers between devices, local(): whole = lax.all_gather(stacked, 'dp', axis=1, tiled=True)  55.1 us
    psum x1, blocking collectives, local(): gain_grad = lax.psum(jnp.sum(d_nlat * normed, axis=0), ('sp', 'dp'))  44 us
    unnamed x5, waiting for transfers between devices  34.6 us
    dot_general x3, matrix products, attend_backward(): jnp.einsum('hqk,qhd->khd', p_b, go, preferred_element_type=f32)  30.3 us
    sub x3, other arithmetic, attend_backward(): probs = jax.nn.softmax(scores, axis=-1)  20.1 us
  transfers between devices with their start and end apart: 7, of which 5 were waited for; matrix products, arithmetic and copies ran while one was open for 10% of the time, Pallas kernels for 0%

commit v1 on v0

--- a/solution.py
+++ b/solution.py
@@ -96,7 +96,8 @@
     normed = lat * inv_rms
     nlat = (normed * latent_norm_gain).astype(bf16)
     stacked = jnp.stack([key_up_matrix, value_up_matrix])
-    whole = lax.all_gather(stacked, "dp", axis=1, tiled=True)
+    blocks = lax.all_gather(stacked, "dp")
+    whole = jnp.concatenate(blocks, axis=1)
     kv_tok = jnp.einsum("tc,gnc->tgn", nlat, whole, preferred_element_type=f32).astype(bf16)
     heads_query = query[0].reshape(tokens, ATTENTION_HEADS, width)
     key_nope = kv_tok[:, 0].reshape(tokens, ATTENTION_HEADS, PLAIN_HEAD_WIDTH)

time: 747 us -> 748 us (level)
  other arithmetic: 59.6 us -> 50.7 us
  local copies, waits for them, and re-layouts: 87 us -> 94.5 us
    convert_element_type x3, other arithmetic: 17 us -> 8.81 us  [attend_backward(): ds_b = d_scores.astype(bf16)]
    all_gather x0 -> x1, local copies, waits for them, and re-layouts: none -> 7.57 us  [local(): blocks = lax.all_gather(stacked, 'dp')]
where the time goes in v1:
time: 748 us; the launch traced here: 737 us
  waiting for transfers between devices  274 us (37%)
  blocking collectives  171 us (23%)
  matrix products  118 us (16%)
  local copies, waits for them, and re-layouts  94.5 us (13%)
  other arithmetic  50.7 us (7%)
  between operations  15 us (2%)
  starting transfers between devices  14.9 us (2%)
    all_gather x1, blocking collectives, local(): rope_full = lax.all_gather(rope_key[0], 'sp', axis=0, tiled=True)  127 us
    psum x1, waiting for transfers between devices, local(): weight_grads = lax.psum(partial_value, 'sp')  103 us
    all_to_all x1, waiting for transfers between devices, local(): lax.all_to_all(grads_heads, 'sp', split_axis=0, concat_axis=1, tiled=True)  64.9 us
    all_gather x1, waiting for transfers between devices, local(): blocks = lax.all_gather(stacked, 'dp')  54.9 us
    psum x1, blocking collectives, local(): gain_grad = lax.psum(jnp.sum(d_nlat * normed, axis=0), ('sp', 'dp'))  44 us
    unnamed x5, waiting for transfers between devices  35.1 us
    dot_general x3, matrix products, attend_backward(): jnp.einsum('hqk,qhd->khd', p_b, go, preferred_element_type=f32)  30.3 us
    sub x3, other arithmetic, attend_backward(): probs = jax.nn.softmax(scores, axis=-1)  20.1 us
  transfers between devices with their start and end apart: 7, of which 5 were waited for; matrix products, arithmetic and copies ran while one was open for 10% of the time, Pallas kernels for 0%

profile of v1, /device:TPU:0, one launch (start us, length us, event | category | flops | bytes accessed | tf_op | source)
XLA Modules:
  0.0 737.4 jit_solution(639299617381466546)
XLA Ops:
  16.6 54.9 %all-gather.7.cloned.1.call-done = bf16[8,512,1024]{2,1,0:T(8,128)(2,1)} async-done(((bf16[2,512,1024]{2,1,0:T(8,128)(2,1)}), bf16[8,512,1024]{2,1,0:T(8,128)(2,1)}) %all-gather.7.cloned.1.call-update) | async-done | bytes 8388624 | tf_op jit(solution)/shard_map/all_gather | solution.py:99
  71.5 7.6 %copy.95 = bf16[4,2,512,1024]{3,2,0,1:T(8,128)(2,1)} copy(bf16[4,2,512,1024]{3,2,1,0:T(8,128)(2,1)} %bitcast.192) | data formatting | bytes 16777216 | tf_op jit(solution)/shard_map/all_gather | solution.py:99
  79.1 6.3 convolution_convert_fusion
  95.4 5.6 pad_maximum_fusion
  101.0 4.0 copy.102
  105.0 5.6 all-to-all-start
  110.8 126.8 %all-gather.1 = bf16[1,1536,32]{2,0,1:T(2,128)(2,1)S(1)} all-gather(bf16[1,192,32]{2,0,1:T(2,128)(2,1)S(1)} %copy.104), channel_id=3, replica_groups=mesh['sp'=8,'dp'=4] {'sp'}, dimensions={1}, use_global_device_ids=true | all-gather | bytes 110592 | tf_op jit(solution)/shard_map/all_gather | solution.py:108
  244.0 8.3 %copy.103 = bf16[8,192,4,288]{1,0,3,2:T(8,128)(2,1)} copy(bf16[8,192,4,288]{3,1,2,0:T(8,128)(2,1)} %bitcast.12) | data formatting | bytes 7077888 | tf_op jit(solution)/shard_map/all_to_all | solution.py:107
  252.4 6.9 all_to_all.42
  265.6 5.4 fusion.43
  300.0 8.5 %fusion.4 = f32[4,512,1536]{2,1,0:T(8,128)} fusion(f32[1536,512,4]{0,1,2:T(8,128)S(1)} %fusion.109, pred[512,1536]{1,0:T(8,128)(4,1)S(1)} %copy-done.12, bf16[1536,4,288]{0,2,1:T(8,128)(2,1)} %copy-done.3), kind=kOutput, calls=%fused_computation.5 | convolution fusion | flops 412090368 | bytes 27000832 | tf_op jit(solution)/shard_map/qhd,khd->hqk/dot_general | solution.py:57
  308.5 14.9 %fusion.149 = (f32[4,512]{1,0:T(4,128)S(1)}, f32[4,512,1536]{2,1,0:T(8,128)}) fusion(f32[4,512,1536]{2,1,0:T(8,128)} %fusion.4), kind=kOutput, calls=%fused_computation.222 | output fusion | flops 6292991 | bytes 25174016 | tf_op jit(solution)/shard_map/sub | solution.py:65
  323.4 11.8 %multiply_reduce_fusion = (f32[4,512]{1,0:T(4,128)S(1)}, f32[4,512,1536]{2,1,0:T(8,128)}) fusion(f32[4,512,1536]{2,1,0:T(8,128)} %get-tuple-element.173, f32[4,512]{1,0:T(4,128)S(1)} %get-tuple-element.172, bf16[1536,4,288]{0,2,1:T(8,128)(2,1)} %copy-done.3), kind=kOutput, calls=%fused_computation.7 | convolution fusion | flops 412088320 | bytes 26230784 | tf_op jit(solution)/shard_map/qhd,khd->hqk/dot_general | solution.py:66
  335.2 6.0 multiply_convert_fusion
  341.3 4.5 fusion.52
  351.1 11.2 %fusion.37 = f32[1536,4,64]{0,2,1:T(8,128)} fusion(f32[1536,4,64]{0,2,1:T(8,128)} %scatter-add.24, bf16[1536,4,288]{0,2,1:T(8,128)(2,1)} %copy-done.3, f32[4,512]{1,0:T(4,128)S(1)} %get-tuple-element.170, f32[4,512,1024]{2,1,0:T(8,128)} %copy-done.2), kind=kOutput, calls=%fused_computation.53 | convolution fusion | flops 274992128 | bytes 19144704 | tf_op jit(solution)/shard_map/hqk,qhd->khd/dot_general | solution.py:81
  362.3 4.4 fusion.42
  366.6 13.7 %fusion.22 = bf16[1536,4,64]{0,2,1:T(8,128)(2,1)} fusion(f32[1536,4,64]{0,2,1:T(8,128)} %fusion.37, bf16[1536,4,288]{0,2,1:T(8,128)(2,1)} %copy-done.3, f32[4,512]{1,0:T(4,128)S(1)} %get-tuple-element.172, f32[4,512,1536]{2,1,0:T(8,128)} %fusion.4), kind=kOutput, calls=%fused_computation.36 | convolution fusion | flops 412880384 | bytes 27795456 | tf_op jit(solution)/shard_map/hqk,qhd->khd/dot_general | solution.py:81
  380.5 4.6 fusion.21
  388.3 5.8 copy.112
  394.1 4.4 all-to-all-start.1
  400.7 64.9 %all-to-all-done.1 = bf16[1536,4,224]{2,1,0:T(4,128)(2,1)} async-done(((bf16[1536,4,224]{2,1,0:T(4,128)(2,1)}), bf16[1536,4,224]{2,1,0:T(4,128)(2,1)}, u32[]{:S(2)}, u32[]{:S(2)}) %all-to-all-start.1) | async-done | bytes 2752544 | tf_op jit(solution)/shard_map/all_to_all | solution.py:110
  483.1 6.1 copy.121
  489.1 4.4 all-to-all-start.2
  503.0 16.3 %all-to-all-done.2 = bf16[1,192,2,2048]{1,2,0,3:T(2,128)(2,1)} async-done(((bf16[1,192,2,2048]{1,2,0,3:T(2,128)(2,1)}), bf16[1,192,2,2048]{1,2,0,3:T(2,128)(2,1)}, u32[]{:S(2)}, u32[]{:S(2)}) %all-to-all-start.2) | async-done | bytes 1572896 | tf_op jit(solution)/shard_map/all_to_all | solution.py:118
  519.3 6.0 copy.123
  525.3 5.7 convolution_bitcast_fusion.1
  531.1 34.6 %reduce-scatter.4.cloned.1.call-done = f32[192,32]{1,0:T(8,128)} async-done(((f32[1536,32]{1,0:T(8,128)}), f32[192,32]{1,0:T(8,128)}) %reduce-scatter.4.cloned.1.call-update) | async-done | bytes 24592
  571.6 6.3 fusion.70
  577.9 44.0 %psum.15 = f32[1024]{0:T(1024)} all-reduce(f32[1024]{0:T(1024)S(1)} %get-tuple-element.138), channel_id=1, replica_groups=mesh['sp'=8,'dp'=4] {'sp','dp'}, use_global_device_ids=true, to_apply=%region_14.15 | all-reduce | flops 1024 | bytes 8192 | tf_op jit(solution)/shard_map/psum | solution.py:121
  623.0 102.6 %all-reduce.5.cloned.1.call-done = f32[2,512,1024]{2,1,0:T(8,128)} async-done(((f32[2,512,1024]{2,1,0:T(8,128)}), f32[2,512,1024]{2,1,0:T(8,128)}) %all-reduce.5.cloned.1.call-update) | async-done | bytes 4194320 | tf_op jit(solution)/shard_map/psum | solution.py:120
  725.6 4.8 slice_bitcast_fusion
  (185 shorter events, 105.4 us)
Async XLA Ops:
  7.2 64.3 %all-gather.7.cloned.1.call-start = ((), (), s32[]{:S(2)}) async-start(), calls=%async_computation.6 | async-start | bytes 10485760 | tf_op jit(solution)/shard_map/all_gather | solution.py:99
  10.3 5.9 copy-start.10
  10.4 6.0 copy-start.41
  16.4 62.7 %copy-start.44 = (f32[192]{0:T(256)}, f32[192]{0:T(256)S(1)}, u32[]{:S(2)}) copy-start(f32[192]{0:T(256)S(1)} %add_rsqrt_fusion) | copy-start | bytes 2308
  16.6 62.5 %copy-start.20 = (bf16[1,192,1024]{2,1,0:T(8,128)(2,1)}, bf16[1,192,1024]{2,1,0:T(8,128)(2,1)S(1)}, u32[]{:S(2)}) copy-start(bf16[1,192,1024]{2,1,0:T(8,128)(2,1)S(1)} %fusion.73) | copy-start | bytes 1179652
  105.0 5.7 copy-start.43
  105.0 139.0 %all-to-all-start = ((bf16[192,32,288]{2,0,1:T(8,128)(2,1)}), bf16[192,32,288]{2,0,1:T(8,128)(2,1)}, u32[]{:S(2)}, u32[]{:S(2)}) async-start(bf16[192,32,288]{2,0,1:T(8,128)(2,1)} %copy.102), calls=%async_computation | async-start | bytes 9437184 | tf_op jit(solution)/shard_map/all_to_all | solution.py:107
  259.2 11.8 %copy-start.3 = (bf16[1536,4,288]{0,2,1:T(8,128)(2,1)}, bf16[1536,4,288]{0,2,1:T(8,128)(2,1)S(1)}, u32[]{:S(2)}) copy-start(bf16[1536,4,288]{0,2,1:T(8,128)(2,1)S(1)} %all_to_all.42) | copy-start | bytes 10616836
  275.6 5.0 copy-start.7
  275.7 5.0 copy-start.9
  292.9 5.2 copy-start.1
  323.4 11.8 %slice-start = ((s8[12582912]{0:T(1024)(128)(4,1)}), s8[4194304]{0:T(1024)(128)(4,1)S(1)}, s32[]{:S(2)}) async-start(s8[12582912]{0:T(1024)(128)(4,1)} %bitcast.185), calls=%async_computation.8 | async-start | bytes 8388608
  323.4 11.8 %slice-start.1 = ((s8[12582912]{0:T(1024)(128)(4,1)}), s8[4194304]{0:T(1024)(128)(4,1)S(1)}, s32[]{:S(2)}) async-start(s8[12582912]{0:T(1024)(128)(4,1)} %bitcast.185), calls=%async_computation.9 | async-start | bytes 8388608
  323.4 11.8 %slice-start.2 = ((s8[12582912]{0:T(1024)(128)(4,1)}), s8[4194304]{0:T(1024)(128)(4,1)S(1)}, s32[]{:S(2)}) async-start(s8[12582912]{0:T(1024)(128)(4,1)} %bitcast.185), calls=%async_computation.10 | async-start | bytes 8388608
  341.3 7.1 copy-start
  380.4 4.8 copy-start.39
  380.4 4.8 copy-start.40
  380.4 4.8 copy-start.22
  380.4 4.8 copy-start.37
  380.4 4.8 copy-start.38
  380.4 4.9 copy-start.23
  380.4 4.9 copy-start.35
  380.4 4.9 copy-start.36
  380.4 4.9 copy-start.25
  380.4 4.9 copy-start.26
  380.4 4.9 copy-start.27
  380.4 4.9 copy-start.33
  394.1 71.5 %all-to-all-start.1 = ((bf16[1536,4,224]{2,1,0:T(4,128)(2,1)}), bf16[1536,4,224]{2,1,0:T(4,128)(2,1)}, u32[]{:S(2)}, u32[]{:S(2)}) async-start(bf16[1536,4,224]{2,1,0:T(4,128)(2,1)} %copy.112), calls=%async_computation.1 | async-start | bytes 6291456 | tf_op jit(solution)/shard_map/all_to_all | solution.py:110
  398.5 126.8 %all-gather.5.cloned.1.call-start = ((), (), s32[]{:S(2)}) async-start(), calls=%async_computation.4 | async-start | bytes 1966080 | tf_op jit(solution)/shard_map/all_gather | solution.py:117
  489.1 30.2 %all-to-all-start.2 = ((bf16[1,192,2,2048]{1,2,0,3:T(2,128)(2,1)}), bf16[1,192,2,2048]{1,2,0,3:T(2,128)(2,1)}, u32[]{:S(2)}, u32[]{:S(2)}) async-start(bf16[1,192,2,2048]{1,2,0,3:T(2,128)(2,1)} %copy.121), calls=%async_computation.2 | async-start | bytes 4194304 | tf_op jit(solution)/shard_map/all_to_all | solution.py:118
  493.6 72.1 %reduce-scatter.4.cloned.1.call-start = ((), (), s32[]{:S(2)}) async-start(), calls=%async_computation.7 | async-start | bytes 884736
  503.0 222.7 %all-reduce.5.cloned.1.call-start = ((), (), s32[]{:S(2)}) async-start(), calls=%async_computation.5 | async-start | bytes 8388608 | tf_op jit(solution)/shard_map/psum | solution.py:120
  (26 other events, 63.1 us)
Sparse Core Ops, SparseCore 0:
  10.5 60.9 all-gather.6
  400.9 19.9 all-gather.4
  503.1 62.5 reduce-scatter.3
  569.2 156.3 all-reduce.4
